TPU v7x, 32 devices: a whole 2x2x4 slice. The times are simulated.
32 devices in a mesh: st: 16 (over z, y, x), tp: 2 (over core).
Axes of the slice: x: 2, y: 2, z: 4, core: 2. Of those that a mesh axis runs over, the one named last changes fastest.
Arguments:
- tokens: bfloat16 [16384, 2048], P('st', 'tp'), may hold values from -6 to 6
- norm_gain: float32 [2048], replicated, may hold values from 0.1 to 1.9
- branch_outer: bfloat16 [2048, 2048], P(None, 'tp'), may hold values from -0.125 to 0.125
- branch_gate: bfloat16 [2048, 2048], P(None, 'tp'), may hold values from -0.125 to 0.125
- branch_input: bfloat16 [2048, 2048], P(None, 'tp'), may hold values from -0.125 to 0.125
- conv_taps: float32 [3, 2048], P(None, 'tp'), may hold values from -3.5 to 3.5
- query_weight: bfloat16 [2048, 1024], P(None, 'tp'), may hold values from -0.125 to 0.125
- query_gain: float32 [128], replicated, may hold values from 0.1 to 1.9
- head_scale: float32 [8], P('tp'), may hold values from 1 to 240
- store: bfloat16 [256, 64, 2048], P('st'), may hold values from -6 to 6
- store_gain: float32 [2048], replicated, may hold values from 0.1 to 1.9
- key_weight: bfloat16 [2048, 256], P(None, 'tp'), may hold values from -0.125 to 0.125
- value_weight: bfloat16 [2048, 256], P(None, 'tp'), may hold values from -0.125 to 0.125
- key_gain: float32 [128], replicated, may hold values from 0.1 to 1.9
- out_weight: bfloat16 [1024, 2048], P(None, 'tp'), may hold values from -0.1875 to 0.1875
- gate_logit: float32 [2048], P('tp'), may hold values from -1 to 4
- passage_ids: int32 [256, 4], P('st'), may hold values from 0 to 255, as said below
Outputs:
- mixed: bfloat16 [16384, 2048], P('st', 'tp')
Inputs may be any that keep to these rules, and one draw needn't show every extreme that they name: `passage_ids`: passage p lies in the rows of store held by index p // 16 of st. Among the ids of the rows of one device (its 16 blocks), at most 4 name passages held by any one device, and exactly 4 name passages of some one device; each device names a passage of the device before it and one of the device half the axis away.
All inputs are finite; a program needn't handle non-finite values.
Results may differ from a plain program's by a relative error of at most 0.006.
The roundings to bfloat16 on the way count: a program that leaves them out, or rounds other values in their place, can miss the bound.
Values may be sent and summed in bfloat16 or wider, within the bound.
A program may use at most 128 MiB of HBM per device.

v0:
```python
import functools
import math

import jax
import jax.numpy as jnp
from jax import lax
from jax.experimental import pallas as pl
from jax.experimental.pallas import tpu as pltpu
from jax.sharding import PartitionSpec as P

MESH = pl.DeviceIdType.MESH
LANES = 128
SEQ = 128
EPS = 1e-06
NT = (((1,), (1,)), ((), ()))
TN = (((0,), (0,)), ((), ()))


def norm_rows(values, gain):
    values = values.astype(jnp.float32)
    return values * lax.rsqrt(jnp.mean(values * values, axis=-1, keepdims=True) + EPS) * gain


def largest(total, options):
    return next(c for c in options if total % c == 0)


def layer_kernel(
    cfg, slots, blocks, head_scale, pick_hbm, tokens_hbm, norm_gain_hbm, outer_hbm, gate_hbm,
    input_hbm, taps_hbm, query_hbm, query_gain_hbm, store_hbm, store_gain_hbm, key_hbm, value_hbm,
    key_gain_hbm,
    attended_hbm, conv_hbm,
    half, normed, outer, gate, inp, query, pair, held, table, mirror_table, send_buf, relay_buf,
    received, q, partials, stats, attended, conv, norm_gain, taps, query_gain, store_gain, key_gain,
    pick_row, picks, wanted,
    store_sem, side_sem, weight_sem, swap_sem, id_send, id_recv, mirror_send, mirror_recv,
    send_sem, relay_sem, recv_sem, conv_sem, part_send, part_recv, out_sem,
):
    n, planes, capacity, per_block, groups, repeat, head_dim, block_rows, relay_after = cfg
    me = lax.axis_index("st")
    core = lax.axis_index("tp")
    plane = n // planes
    level, place = me // plane, lax.rem(me, plane)
    relays = planes == 4
    middle = (level == 1) | (level == 2)
    mirror = (planes - 1 - level) * plane + place
    levels = [level]
    if relays:
        levels = [
            level,
            level + 1 - 2 * lax.rem(level, 2),
            level + 2 - 4 * lax.rem(level // 2, 2),
            3 - level,
        ]
    near = (0, 1) if relays else (0,)
    far = (2, 3) if relays else ()

    def peer(step, j):
        return levels[step] * plane + lax.rem(place + j, plane)

    def every(body, steps=near + far, own=False):
        for step in steps:

            def run(j, carry, step=step):
                body(step, j)
                return carry

            lax.fori_loop(1 if step == 0 and not own else 0, plane, run, 0)

    chunks, chunk_rows = held.shape[0], held.shape[1]
    passage_rows = table.shape[1]
    chunk_passages = chunk_rows // passage_rows
    key_width = key_hbm.shape[1]
    token_rows = tokens_hbm.shape[0]

    def load(c):
        return pltpu.make_async_copy(
            store_hbm.at[pl.ds(c * chunk_rows, chunk_rows)], held.at[c], store_sem.at[c]
        )

    sides = [
        pltpu.make_async_copy(source, target, side_sem.at[k])
        for k, (source, target) in enumerate(
            [
                (store_gain_hbm, store_gain),
                (key_hbm, pair.at[:, pl.ds(0, key_width)]),
                (value_hbm, pair.at[:, pl.ds(key_width, value_hbm.shape[1])]),
                (key_gain_hbm, key_gain),
                (pick_hbm, pick_row),
                (pick_hbm, picks.at[me]),
                (norm_gain_hbm, norm_gain),
                (query_gain_hbm, query_gain),
                (taps_hbm, taps),
                (tokens_hbm, half.at[core]),
            ]
        )
    ]
    weights = [
        pltpu.make_async_copy(source, target, weight_sem.at[k])
        for k, (source, target) in enumerate(
            [(query_hbm, query), (gate_hbm, gate), (input_hbm, inp), (outer_hbm, outer)]
        )
    ]

    def remote(source, target, sent, got, to):
        return pltpu.make_async_remote_copy(
            src_ref=source,
            dst_ref=target,
            send_sem=sent,
            recv_sem=got,
            device_id=to,
            device_id_type=MESH,
        )

    across = {"tp": 1 - core}
    swap_tokens = remote(tokens_hbm, half.at[core], swap_sem.at[0], swap_sem.at[1], across)

    def send_ids(step, j):
        to = peer(step, j)
        return remote(pick_row, picks.at[me], id_send.at[to], id_recv.at[me], {"st": to})

    def take_ids(step, j):
        owner = peer(step, j)
        return remote(pick_row, picks.at[owner], id_send.at[owner], id_recv.at[owner], {"st": owner})

    def swap_table(c):
        at = pl.ds(c * chunk_passages, chunk_passages)
        return remote(
            table.at[at], mirror_table.at[at], mirror_send.at[c], mirror_recv.at[c], {"st": mirror}
        )

    def wants(to, owner):
        return [wanted[to, 0, owner * capacity + r] for r in range(capacity)]

    def fill(step, j):
        to = peer(step, j)
        for r, pick in enumerate(wants(to, me)):
            send_buf[to * capacity + r] = table[pick]

    def send(step, j):
        to = peer(step, j)
        return remote(
            send_buf.at[pl.ds(to * capacity, capacity)],
            received.at[pl.ds(me * capacity, capacity)],
            send_sem.at[to],
            recv_sem.at[me],
            {"st": to},
        )

    def take(step, j):
        owner = peer(step, j)
        return remote(
            send_buf.at[pl.ds(owner * capacity, capacity)],
            received.at[pl.ds(owner * capacity, capacity)],
            send_sem.at[owner],
            recv_sem.at[owner],
            {"st": owner},
        )

    def fill_relay(step, j):
        at = (step * plane + j) * capacity
        for r, pick in enumerate(wants(peer(step, j), mirror)):
            relay_buf[at + r] = mirror_table[pick]

    def relay(step, j):
        k = step * plane + j
        return remote(
            relay_buf.at[pl.ds(k * capacity, capacity)],
            received.at[pl.ds(mirror * capacity, capacity)],
            relay_sem.at[k],
            recv_sem.at[mirror],
            {"st": peer(step, j)},
        )

    def project(c):
        load(c).wait()
        memory = norm_rows(held[c], store_gain[...]).astype(jnp.bfloat16)
        raw = jnp.dot(memory, pair[...], preferred_element_type=jnp.float32)
        keys = [
            norm_rows(raw[:, g * head_dim : (g + 1) * head_dim], key_gain[...])
            for g in range(groups)
        ]
        done = jnp.concatenate(keys + [raw[:, groups * head_dim :]], axis=1).astype(jnp.bfloat16)
        table[pl.ds(c * chunk_passages, chunk_passages)] = done.reshape(
            chunk_passages, passage_rows, done.shape[1]
        )

    load(0).start()
    for side in sides[:-1]:
        side.start()
    for c in range(1, chunks):
        load(c).start()
    barrier = pltpu.get_barrier_semaphore()

    def greet(step, j):
        pl.semaphore_signal(barrier, inc=1, device_id={"st": peer(step, j)}, device_id_type=MESH)

    every(greet)
    pl.semaphore_signal(barrier, inc=1, device_id=across, device_id_type=MESH)
    for k in range(4):
        sides[k].wait()
    for c in range(chunks):
        project(c)
        if c == 0:
            sides[4].wait()
            pl.semaphore_wait(barrier, n)
            every(lambda step, j: send_ids(step, j).start())
            sides[-1].start()
            swap_tokens.start()
        if relays and c > 0:

            @pl.when(middle)
            def _(c=c):
                swap_table(c - 1).start()

    for weight in weights:
        weight.start()
    if relays:

        @pl.when(middle)
        def _():
            swap_table(chunks - 1).start()

    for side in sides[5:-1]:
        side.wait()
    every(lambda step, j: take_ids(step, j).wait_recv())
    listed = pltpu.make_async_copy(picks, wanted, side_sem.at[len(sides)])
    listed.start()
    listed.wait()
    every(fill, near)
    if relays:

        @pl.when(jnp.logical_not(middle))
        def _():
            every(fill, far)

    every(lambda step, j: send(step, j).start(), near)
    if relays:

        @pl.when(jnp.logical_not(middle))
        def _():
            every(lambda step, j: send(step, j).start(), far)

    for r, pick in enumerate(wants(me, me)):
        received[me * capacity + r] = table[pick]

    sides[-1].wait()
    swap_tokens.wait()
    norm_tile = largest(token_rows, (128, 64, 32, 16, 8))

    def normalize(i, carry):
        rows = pl.ds(pl.multiple_of(i * norm_tile, norm_tile), norm_tile)
        whole = jnp.concatenate([half[0, rows, :], half[1, rows, :]], axis=1)
        normed[rows, :] = norm_rows(whole, norm_gain[...]).astype(jnp.bfloat16)
        return carry

    lax.fori_loop(0, token_rows // norm_tile, normalize, 0)

    weights[0].wait()
    tile_blocks = largest(token_rows // block_rows, (4, 2, 1))
    tile_rows = tile_blocks * block_rows

    def ask(i, carry):
        rows = pl.ds(pl.multiple_of(i * tile_rows, tile_rows), tile_rows)
        raw = jnp.dot(normed[rows, :], query[...], preferred_element_type=jnp.float32)
        for g in range(groups):
            for h in range(repeat):
                at = (g * repeat + h) * head_dim
                scale = head_scale[g * repeat + h] * (1.0 / math.sqrt(head_dim))
                head = norm_rows(raw[:, at : at + head_dim], query_gain[...]) * scale
                head = head.astype(jnp.bfloat16)
                for b in range(tile_blocks):
                    q[(i * tile_blocks + b) * groups + g, pl.ds(h * block_rows, block_rows), :] = (
                        head[b * block_rows : (b + 1) * block_rows]
                    )
        return carry

    lax.fori_loop(0, token_rows // tile_rows, ask, 0)

    for weight in weights[1:]:
        weight.wait()
    conv_rows = largest(token_rows // SEQ, (4, 2, 1)) * SEQ
    conv_columns = largest(conv.shape[1] // LANES, (2, 1)) * LANES
    across_tiles = conv.shape[1] // conv_columns
    down_tiles = token_rows // conv_rows
    conv_tiles = across_tiles * down_tiles

    def conv_out(t):
        c, i = t // down_tiles, lax.rem(t, down_tiles)
        rows = pl.ds(pl.multiple_of(i * conv_rows, conv_rows), conv_rows)
        columns = pl.ds(pl.multiple_of(c * conv_columns, conv_columns), conv_columns)
        return pltpu.make_async_copy(
            conv.at[rows, columns], conv_hbm.at[rows, columns], conv_sem.at[t]
        )

    def branch(t, carry):
        c, i = t // down_tiles, lax.rem(t, down_tiles)
        rows = pl.ds(pl.multiple_of(i * conv_rows, conv_rows), conv_rows)
        columns = pl.ds(pl.multiple_of(c * conv_columns, conv_columns), conv_columns)
        left = normed[rows, :]
        z = jnp.dot(left, gate[:, columns], preferred_element_type=jnp.float32)
        z = z * jnp.dot(left, inp[:, columns], preferred_element_type=jnp.float32)
        at = lax.rem(lax.broadcasted_iota(jnp.int32, (conv_rows, 1), 0), SEQ)
        one = jnp.where(at < 1, 0.0, pltpu.roll(z, 1, 0))
        two = jnp.where(at < 2, 0.0, pltpu.roll(z, 2, 0))
        summed = (
            two * taps[0:1, columns] + one * taps[1:2, columns] + z * taps[2:3, columns]
        )
        conv[rows, columns] = (
            jnp.dot(left, outer[:, columns], preferred_element_type=jnp.float32) * summed
        )
        conv_out(t).start()
        return carry

    before = min(conv_tiles, relay_after) if relays else conv_tiles
    lax.fori_loop(0, before, branch, 0)
    if relays:

        @pl.when(middle)
        def _():
            for c in range(chunks):
                swap_table(c).wait()
            every(fill_relay, near, own=False)
            every(lambda step, j: relay(step, j).start(), near)
            for r, pick in enumerate(wants(me, mirror)):
                received[mirror * capacity + r] = mirror_table[pick]

        lax.fori_loop(before, conv_tiles, branch, 0)

    width = repeat * block_rows

    def attend(step, j):
        owner = peer(step, j)
        if step == 0:

            @pl.when(j > 0)
            def _():
                take(step, j).wait_recv()
        elif step == 3:

            @pl.when(jnp.logical_not(middle & (j == 0)))
            def _():
                take(step, j).wait_recv()
        else:
            take(step, j).wait_recv()
        for r in range(capacity):
            slot = owner * capacity + r
            block = blocks[slot]
            for g in range(groups):
                passage = received[slot]
                asked = q[block * groups + g]
                key = passage[:, g * head_dim : (g + 1) * head_dim]
                value = passage[:, (groups + g) * head_dim : (groups + g + 1) * head_dim]
                scores = lax.dot_general(key, asked, NT, preferred_element_type=jnp.float32)
                top = jnp.max(scores, axis=0, keepdims=True)
                weight = jnp.exp(scores - top)
                total = jnp.sum(weight, axis=0, keepdims=True)
                shares = (weight * (1.0 / total)).astype(jnp.bfloat16)
                part = lax.dot_general(value, shares, TN, preferred_element_type=jnp.float32)
                partials[slot * groups + g] = part.astype(jnp.bfloat16)
                stats[slot * groups + g, 0:1, :] = top
                stats[slot * groups + g, 1:2, :] = total

    every(attend, own=True)

    block_count = token_rows // block_rows
    parts = part_send.shape[0]
    part_blocks = block_count // parts
    part_rows = part_blocks * block_rows

    def swap_part(k):
        here = attended.at[core, pl.ds(k * part_rows, part_rows)]
        return remote(here, here, part_send.at[k], part_recv.at[k], across)

    def combine(b, carry):
        for g in range(groups):
            at = [slots[b * per_block + p] * groups + g for p in range(per_block)]
            tops = [stats[s, 0:1, :] for s in at]
            highest = functools.reduce(jnp.maximum, tops)
            scales = [jnp.exp(top - highest) * stats[s, 1:2, :] for top, s in zip(tops, at)]
            denominator = functools.reduce(jnp.add, scales)
            summed = functools.reduce(
                jnp.add, [partials[s].astype(jnp.float32) * scale for s, scale in zip(at, scales)]
            )
            done = jnp.transpose(summed * (1.0 / denominator)).astype(jnp.bfloat16)
            rows = pl.ds(pl.multiple_of(b * block_rows, block_rows), block_rows)
            for h in range(repeat):
                columns = slice((g * repeat + h) * head_dim, (g * repeat + h + 1) * head_dim)
                attended[core, rows, columns] = done[h * block_rows : (h + 1) * block_rows]
        return carry

    for k in range(parts):
        lax.fori_loop(k * part_blocks, (k + 1) * part_blocks, combine, 0)
        if k > 0:
            swap_part(k - 1).start()
    swap_part(parts - 1).start()

    def leave(index, side):
        wide = attended.shape[2]
        return pltpu.make_async_copy(
            attended.at[side],
            attended_hbm.at[:, pl.ds(pl.multiple_of(side * wide, LANES), wide)],
            out_sem.at[index],
        )

    leave(0, core).start()
    every(lambda step, j: send_ids(step, j).wait_send())
    every(lambda step, j: send(step, j).wait_send(), near)
    if relays:

        @pl.when(middle)
        def _():
            every(lambda step, j: relay(step, j).wait_send(), near)

        @pl.when(jnp.logical_not(middle))
        def _():
            every(lambda step, j: send(step, j).wait_send(), far)

    def landed(t, carry):
        conv_out(t).wait()
        return carry

    lax.fori_loop(0, conv_tiles, landed, 0)
    for k in range(parts):
        swap_part(k).wait()
    leave(1, 1 - core).start()
    leave(0, core).wait()
    leave(1, 1 - core).wait()


def on_device(
    planes,
    tokens,
    norm_gain,
    branch_outer,
    branch_gate,
    branch_input,
    conv_taps,
    query_weight,
    query_gain,
    head_scale,
    store,
    store_gain,
    key_weight,
    value_weight,
    key_gain,
    out_weight,
    gate_logit,
    passage_ids,
):
    n = lax.axis_size("st")
    token_rows, local_width = tokens.shape
    head_dim = query_gain.shape[0]
    local_heads = query_weight.shape[1] // head_dim
    groups = key_weight.shape[1] // head_dim
    repeat = local_heads // groups
    block_count, per_block = passage_ids.shape
    block_rows = token_rows // block_count
    passages, passage_rows, width = store.shape
    channels = branch_outer.shape[1]
    requests = block_count * per_block
    capacity = max(2, (requests + n - 1) // n)
    count = n * capacity
    flat = passage_ids.reshape(requests)
    owners = flat // passages
    order = jnp.arange(requests, dtype=jnp.int32)
    earlier = (owners[:, None] == owners[None, :]) & (order[None, :] < order[:, None])
    slots = owners * capacity + jnp.sum(earlier.astype(jnp.int32), axis=1)
    lanes = LANES * ((count + LANES - 1) // LANES)
    filled = slots[None, :] == jnp.arange(lanes, dtype=jnp.int32)[:, None]
    pick = jnp.sum(jnp.where(filled, (flat - owners * passages)[None], 0), axis=1)
    blocks = jnp.sum(jnp.where(filled, (order // per_block)[None], 0), axis=1)

    rows = passages * passage_rows
    chunks = largest(passages, (4, 2, 1))
    parts = largest(block_count, (4, 2, 1))
    pair_width = key_weight.shape[1] + value_weight.shape[1]
    wide = repeat * block_rows
    conv_tiles = (token_rows // (largest(token_rows // SEQ, (4, 2, 1)) * SEQ)) * (
        channels // (largest(channels // LANES, (2, 1)) * LANES)
    )
    plane = n // planes
    relays = planes == 4
    bf16, f32 = jnp.bfloat16, jnp.float32
    dma = pltpu.SemaphoreType.DMA
    smem = pl.BlockSpec(memory_space=pltpu.SMEM)
    anywhere = pl.BlockSpec(memory_space=pl.ANY)
    cfg = (n, planes, capacity, per_block, groups, repeat, head_dim, block_rows, RELAY_AFTER)
    attended, conv = pl.pallas_call(
        functools.partial(layer_kernel, cfg),
        out_shape=(
            jax.ShapeDtypeStruct((token_rows, 2 * local_heads * head_dim), bf16),
            jax.ShapeDtypeStruct((token_rows, channels), f32),
        ),
        in_specs=[smem] * 3 + [anywhere] * 14,
        out_specs=(anywhere, anywhere),
        scratch_shapes=[
            pltpu.VMEM((2, token_rows, local_width), bf16),
            pltpu.VMEM((token_rows, width), bf16),
            pltpu.VMEM((width, channels), bf16),
            pltpu.VMEM((width, channels), bf16),
            pltpu.VMEM((width, channels), bf16),
            pltpu.VMEM(query_weight.shape, bf16),
            pltpu.VMEM((width, pair_width), bf16),
            pltpu.VMEM((chunks, rows // chunks, width), bf16),
            pltpu.VMEM((passages, passage_rows, pair_width), bf16),
            pltpu.VMEM((passages, passage_rows, pair_width), bf16),
            pltpu.VMEM((count, passage_rows, pair_width), bf16),
            pltpu.VMEM((2 * plane * capacity if relays else 1, passage_rows, pair_width), bf16),
            pltpu.VMEM((count, passage_rows, pair_width), bf16),
            pltpu.VMEM((block_count * groups, wide, head_dim), bf16),
            pltpu.VMEM((count * groups, head_dim, wide), bf16),
            pltpu.VMEM((count * groups, 2, wide), f32),
            pltpu.VMEM((2, token_rows, local_heads * head_dim), bf16),
            pltpu.VMEM((token_rows, channels), f32),
            pltpu.VMEM((1, width), f32),
            pltpu.VMEM(conv_taps.shape, f32),
            pltpu.VMEM((1, head_dim), f32),
            pltpu.VMEM((1, width), f32),
            pltpu.VMEM((1, head_dim), f32),
            pltpu.VMEM((1, lanes), jnp.int32),
            pltpu.VMEM((n, 1, lanes), jnp.int32),
            pltpu.SMEM((n, 1, lanes), jnp.int32),
            dma((chunks,)),
            dma((11,)),
            dma((4,)),
            dma((2,)),
            dma((n,)),
            dma((n,)),
            dma((chunks,)),
            dma((chunks,)),
            dma((n,)),
            dma((2 * plane,)),
            dma((n,)),
            dma((conv_tiles,)),
            dma((parts,)),
            dma((parts,)),
            dma((2,)),
        ],
        compiler_params=pltpu.CompilerParams(
            collective_id=0, has_side_effects=True, vmem_limit_bytes=62 * 1024 * 1024
        ),
        cost_estimate=pl.CostEstimate(
            flops=2 * token_rows * width * (3 * channels + local_heads * head_dim),
            bytes_accessed=8 * width * channels,
            transcendentals=0,
        ),
        name="layer",
    )(
        slots,
        blocks,
        head_scale,
        pick[None],
        tokens,
        norm_gain[None],
        branch_outer,
        branch_gate,
        branch_input,
        conv_taps,
        query_weight,
        query_gain[None],
        store.reshape(rows, width),
        store_gain[None],
        key_weight,
        value_weight,
        key_gain[None],
    )
    cross = jnp.dot(attended, out_weight, preferred_element_type=jnp.float32)
    mixed = conv + jax.nn.sigmoid(gate_logit) * cross
    return mixed.astype(jnp.bfloat16)


RELAY_AFTER = 4


def planes_of(mesh):
    line = mesh.devices.reshape(mesh.shape["st"], -1)[:, 0]
    heights = [getattr(d, "coords", (0, 0, 0))[2] for d in line]
    planes = len(set(heights))
    plane = len(heights) // planes
    ordered = heights == [h for h in sorted(set(heights)) for _ in range(plane)]
    return planes if planes == 4 and ordered else 1


def solution(mesh):
    return jax.shard_map(
        functools.partial(on_device, planes_of(mesh)),
        mesh=mesh,
        in_specs=(
            P("st", "tp"),
            P(),
            P(None, "tp"),
            P(None, "tp"),
            P(None, "tp"),
            P(None, "tp"),
            P(None, "tp"),
            P(),
            P("tp"),
            P("st", None, None),
            P(),
            P(None, "tp"),
            P(None, "tp"),
            P(),
            P(None, "tp"),
            P("tp"),
            P("st", None),
        ),
        out_specs=P("st", "tp"),
        check_vma=False,
    )
```

profile of v0, /device:TPU:1, one launch (start us, length us, event | category | flops | bytes accessed | tf_op | source)
XLA Modules:
  0.0 69.1 jit_solution(14103298857449263346)
XLA Ops:
  0.0 0.7 %add_divide_fusion = f32[1024]{0:T(1024)S(1)} fusion(f32[1024]{0:T(1024)} %param.32), kind=kLoop, calls=%fused_computation.7 | loop fusion | flops 3072 | bytes 8192 | tf_op jit(solution)/shard_map/div | solution.py:569
  0.7 0.8 %copy.20 = s32[16,4]{1,0:T(8,128)S(1)} copy(s32[16,4]{0,1:T(4,128)} %param.33) | data formatting | bytes 512 | tf_op args[16]
  1.5 0.1 reshape.103
  1.6 0.2 convert_reduce_fusion
  1.8 0.0 copy-start
  1.8 0.6 select_reduce_fusion
  2.4 0.0 copy-done
  2.4 59.5 %layer.1 = (bf16[1024,1024]{1,0:T(8,128)(2,1)}, f32[1024,1024]{1,0:T(8,128)}) custom-call(s32[64]{0:T(128)} %copy-done, s32[128]{0:T(128)} %get-tuple-element.10.blocks, f32[4]{0:T(128)} %head_scale.1, s32[1,128]{1,0:T(1,128)} %bitcast.8, bf16[1024,1024]{1,0:T(8,128)(2,1)} %tokens_hbm.1, f32[1,2048]{1,0:T(1,128)} %bitcast.10, bf16[2048,1024]{1,0:T(8,128)(2,1)} %outer_hbm.1, ...), custom_call_target="tpu_custom_call" | custom-call | flops 15032385536 | bytes 16777216 | tf_op jit(solution)/shard_map/layer/pallas_call | solution.py:489
  61.9 7.1 %add_convert_fusion = bf16[1024,1024]{1,0:T(8,128)(2,1)} fusion(f32[1024,1024]{1,0:T(8,128)} %get-tuple-element.7, bf16[1024,1024]{1,0:T(8,128)(2,1)} %get-tuple-element.8, bf16[1024,1024]{1,0:T(8,128)(2,1)} %param.31, f32[1024]{0:T(1024)S(1)} %add_divide_fusion), kind=kOutput, calls=%fused_computation | convolution fusion | flops 2150629376 | bytes 10489856 | tf_op jit(solution)/shard_map/dot_general | solution.py:568
  (2 shorter events, 0.0 us)
Async XLA Ops:
  1.8 0.7 copy-start
where the time goes:
time: 69.5 us; the launch traced here: 69.1 us
  Pallas kernels  59.5 us (86%)
  matrix products  7.11 us (10%)
  other arithmetic  1.53 us (2%)
  local copies, waits for them, and re-layouts  0.86 us (1%)
    pallas_call x1, Pallas kernels, on_device(): pl.pallas_call(functools.partial(layer_kernel, cfg), out_shape=(jax.Shape...  59.5 us
    dot_general x1, matrix products, on_device(): cross = jnp.dot(attended, out_weight, preferred_element_type=jnp.float32)  7.11 us

commit v1 on v0

v1 whole, which is shorter than its diff:
```python
import functools
import math

import jax
import jax.numpy as jnp
from jax import lax
from jax.experimental import pallas as pl
from jax.experimental.pallas import tpu as pltpu
from jax.sharding import PartitionSpec as P

MESH = pl.DeviceIdType.MESH
LANES = 128
SEQ = 128
EPS = 1e-06
NN = (((1,), (0,)), ((), ()))
TN = (((0,), (0,)), ((), ()))


def norm_rows(values, gain):
    values = values.astype(jnp.float32)
    return values * lax.rsqrt(jnp.mean(values * values, axis=-1, keepdims=True) + EPS) * gain


def largest(total, options):
    return next(c for c in options if total % c == 0)


def layer_kernel(
    cfg, slots, blocks, head_scale, pick_hbm, tokens_hbm, norm_gain_hbm, outer_hbm, gate_hbm,
    input_hbm, taps_hbm, query_hbm, query_gain_hbm, store_hbm, store_gain_hbm, key_hbm, value_hbm,
    key_gain_hbm, out_weight_hbm, gate_logit_hbm,
    mixed_hbm,
    half, normed, outer, gate, inp, query, out_weight, pair, held, own_table, side_table, next_table,
    send_buf, received, q, partials, stats, attended, conv, norm_gain, taps, query_gain, store_gain, key_gain,
    gate_logit, pick_row, picks, wanted,
    store_sem, side_sem, weight_sem, swap_sem, id_send, id_recv, table_send, table_recv,
    send_sem, recv_sem, part_send, part_recv, out_sem,
):
    n, planes, capacity, per_block, groups, repeat, head_dim, block_rows = cfg
    me = lax.axis_index("st")
    core = lax.axis_index("tp")
    plane = n // planes
    level, place = me // plane, lax.rem(me, plane)
    relays = planes == 4
    middle = (level == 1) | (level == 2)
    edge = jnp.logical_not(middle)
    levels = [level]
    if relays:
        half_up = level // 2
        levels += [level + 1 - 2 * lax.rem(level, 2), 2 - half_up, 3 - 3 * half_up]
    beside = [at * plane + place for at in levels]

    def peer(step, j):
        return levels[step] * plane + lax.rem(place + j, plane)

    def every(body, steps, own=False):
        for step in steps:

            def run(j, carry, step=step):
                body(step, j)
                return carry

            lax.fori_loop(1 if step == 0 and not own else 0, plane, run, 0)

    steps = tuple(range(len(levels)))
    tables = [own_table, side_table, next_table]

    chunks, chunk_rows = held.shape[0], held.shape[1]
    passage_rows = own_table.shape[1]
    chunk_passages = chunk_rows // passage_rows
    key_width = key_hbm.shape[1]
    token_rows = tokens_hbm.shape[0]

    def load(c):
        return pltpu.make_async_copy(
            store_hbm.at[pl.ds(c * chunk_rows, chunk_rows)], held.at[c], store_sem.at[c]
        )

    sides = [
        pltpu.make_async_copy(source, target, side_sem.at[k])
        for k, (source, target) in enumerate(
            [
                (store_gain_hbm, store_gain),
                (key_hbm, pair.at[:, pl.ds(0, key_width)]),
                (value_hbm, pair.at[:, pl.ds(key_width, value_hbm.shape[1])]),
                (key_gain_hbm, key_gain),
                (pick_hbm, pick_row),
                (pick_hbm, picks.at[me]),
                (norm_gain_hbm, norm_gain),
                (query_gain_hbm, query_gain),
                (taps_hbm, taps),
                (gate_logit_hbm, gate_logit),
                (tokens_hbm, half.at[core]),
            ]
        )
    ]
    weights = [
        pltpu.make_async_copy(source, target, weight_sem.at[k])
        for k, (source, target) in enumerate(
            [
                (query_hbm, query),
                (gate_hbm, gate),
                (input_hbm, inp),
                (outer_hbm, outer),
                (out_weight_hbm, out_weight),
            ]
        )
    ]

    def remote(source, target, sent, got, to):
        return pltpu.make_async_remote_copy(
            src_ref=source,
            dst_ref=target,
            send_sem=sent,
            recv_sem=got,
            device_id=to,
            device_id_type=MESH,
        )

    across = {"tp": 1 - core}
    swap_tokens = remote(tokens_hbm, half.at[core], swap_sem.at[0], swap_sem.at[1], across)

    def send_ids(step, j):
        to = peer(step, j)
        return remote(pick_row, picks.at[me], id_send.at[to], id_recv.at[me], {"st": to})

    def take_ids(step, j):
        owner = peer(step, j)
        return remote(pick_row, picks.at[owner], id_send.at[owner], id_recv.at[owner], {"st": owner})

    def hand(kind, c):
        at = pl.ds(c * chunk_passages, chunk_passages)
        source, target, to = [(0, 1, 1), (0, 2, 2), (2, 2, 1)][kind]
        return remote(
            tables[source].at[at],
            tables[target].at[at],
            table_send.at[kind, c],
            table_recv.at[target - 1, c],
            {"st": beside[to]},
        )

    def wants(to, owner):
        return [wanted[to, 0, owner * capacity + r] for r in range(capacity)]

    def fill(kind):
        def body(step, j):
            to = peer(step, j)
            at = ((kind if step == 0 else 1 + step) * plane + j) * capacity
            for r, pick in enumerate(wants(to, beside[kind])):
                send_buf[at + r] = tables[kind][pick]

        return body

    def send(kind):
        def body(step, j):
            k = (kind if step == 0 else 1 + step) * plane + j
            owner = beside[kind]
            return remote(
                send_buf.at[pl.ds(k * capacity, capacity)],
                received.at[pl.ds(owner * capacity, capacity)],
                send_sem.at[k],
                recv_sem.at[owner],
                {"st": peer(step, j)},
            )

        return body

    def take(step, j):
        owner = peer(step, j)
        return remote(
            send_buf.at[pl.ds(0, capacity)],
            received.at[pl.ds(owner * capacity, capacity)],
            send_sem.at[0],
            recv_sem.at[owner],
            {"st": owner},
        )

    def serve(kind):
        every(fill(kind), (0,))
        every(lambda step, j: send(kind)(step, j).start(), (0,))
        owner = beside[kind]
        for r, pick in enumerate(wants(me, owner)):
            received[owner * capacity + r] = tables[kind][pick]

    def project(c):
        load(c).wait()
        memory = norm_rows(held[c], store_gain[...]).astype(jnp.bfloat16)
        raw = jnp.dot(memory, pair[...], preferred_element_type=jnp.float32)
        keys = [
            norm_rows(raw[:, g * head_dim : (g + 1) * head_dim], key_gain[...])
            for g in range(groups)
        ]
        done = jnp.concatenate(keys + [raw[:, groups * head_dim :]], axis=1).astype(jnp.bfloat16)
        own_table[pl.ds(c * chunk_passages, chunk_passages)] = done.reshape(
            chunk_passages, passage_rows, done.shape[1]
        )

    load(0).start()
    for side in sides[:-1]:
        side.start()
    for c in range(1, chunks):
        load(c).start()
    barrier = pltpu.get_barrier_semaphore()

    def greet(step, j):
        pl.semaphore_signal(barrier, inc=1, device_id={"st": peer(step, j)}, device_id_type=MESH)

    every(greet, steps)
    pl.semaphore_signal(barrier, inc=1, device_id=across, device_id_type=MESH)

    def hand_on(c):
        if relays:
            hand(0, c).start()

            @pl.when(middle)
            def _():
                hand(1, c).start()

    for k in range(4):
        sides[k].wait()
    for c in range(chunks):
        project(c)
        if c == 0:
            sides[4].wait()
            pl.semaphore_wait(barrier, n)
            every(lambda step, j: send_ids(step, j).start(), steps)
            sides[-1].start()
            swap_tokens.start()
        else:
            hand_on(c - 1)
    for weight in weights:
        weight.start()
    hand_on(chunks - 1)
    for side in sides[5:-1]:
        side.wait()
    every(lambda step, j: take_ids(step, j).wait_recv(), steps)
    listed = pltpu.make_async_copy(picks, wanted, side_sem.at[len(sides)])
    listed.start()
    listed.wait()
    if relays:

        @pl.when(edge)
        def _():
            every(fill(0), (2, 3))
            every(lambda step, j: send(0)(step, j).start(), (2, 3))

    serve(0)

    sides[-1].wait()
    swap_tokens.wait()
    norm_tile = largest(token_rows, (128, 64, 32, 16, 8))

    def normalize(i, carry):
        rows = pl.ds(pl.multiple_of(i * norm_tile, norm_tile), norm_tile)
        whole = jnp.concatenate([half[0, rows, :], half[1, rows, :]], axis=1)
        normed[rows, :] = norm_rows(whole, norm_gain[...]).astype(jnp.bfloat16)
        return carry

    lax.fori_loop(0, token_rows // norm_tile, normalize, 0)

    weights[0].wait()
    tile_blocks = largest(token_rows // block_rows, (4, 2, 1))
    tile_rows = tile_blocks * block_rows

    def ask(i, carry):
        rows = pl.ds(pl.multiple_of(i * tile_rows, tile_rows), tile_rows)
        raw = jnp.dot(normed[rows, :], query[...], preferred_element_type=jnp.float32)
        for g in range(groups):
            heads = []
            for h in range(repeat):
                at = (g * repeat + h) * head_dim
                scale = head_scale[g * repeat + h] * (1.0 / math.sqrt(head_dim))
                head = norm_rows(raw[:, at : at + head_dim], query_gain[...]) * scale
                heads.append(head.astype(jnp.bfloat16))
            for b in range(tile_blocks):
                rows = slice(b * block_rows, (b + 1) * block_rows)
                asked = jnp.concatenate([head[rows] for head in heads], axis=0)
                q[(i * tile_blocks + b) * groups + g] = jnp.transpose(asked)
        return carry

    lax.fori_loop(0, token_rows // tile_rows, ask, 0)

    for weight in weights[1:]:
        weight.wait()
    conv_rows = largest(token_rows // SEQ, (4, 2, 1)) * SEQ
    conv_columns = largest(conv.shape[1] // LANES, (2, 1)) * LANES
    down_tiles = token_rows // conv_rows
    conv_tiles = conv.shape[1] // conv_columns * down_tiles

    def branch(t, carry):
        c, i = t // down_tiles, lax.rem(t, down_tiles)
        rows = pl.ds(pl.multiple_of(i * conv_rows, conv_rows), conv_rows)
        columns = pl.ds(pl.multiple_of(c * conv_columns, conv_columns), conv_columns)
        left = normed[rows, :]
        z = jnp.dot(left, gate[:, columns], preferred_element_type=jnp.float32)
        z = z * jnp.dot(left, inp[:, columns], preferred_element_type=jnp.float32)
        at = lax.rem(lax.broadcasted_iota(jnp.int32, (conv_rows, 1), 0), SEQ)
        one = jnp.where(at < 1, 0.0, pltpu.roll(z, 1, 0))
        two = jnp.where(at < 2, 0.0, pltpu.roll(z, 2, 0))
        summed = (
            two * taps[0:1, columns] + one * taps[1:2, columns] + z * taps[2:3, columns]
        )
        conv[rows, columns] = (
            jnp.dot(left, outer[:, columns], preferred_element_type=jnp.float32) * summed
        )
        return carry

    if relays:

        @pl.when(middle)
        def _():
            for c in range(chunks):
                hand(1, c).wait_recv()
                hand(2, c).start()
            for c in range(chunks):
                hand(0, c).wait_recv()
            serve(1)
            serve(2)

        first, second = conv_tiles * FIRST // 8, conv_tiles * SECOND // 8
        lax.fori_loop(0, first, branch, 0)

        @pl.when(edge)
        def _():
            for c in range(chunks):
                hand(0, c).wait_recv()
            serve(1)

        lax.fori_loop(first, second, branch, 0)

        @pl.when(edge)
        def _():
            for c in range(chunks):
                hand(2, c).wait_recv()
            serve(2)

        lax.fori_loop(second, conv_tiles, branch, 0)
    else:
        lax.fori_loop(0, conv_tiles, branch, 0)

    def attend(step, j):
        owner = peer(step, j)
        if step == 3:
            take(step, j).wait_recv()
        else:

            @pl.when(j > 0)
            def _():
                take(step, j).wait_recv()

        at = [owner * capacity + r for r in range(capacity)]
        for g in range(groups):
            key = slice(g * head_dim, (g + 1) * head_dim)
            value = slice((groups + g) * head_dim, (groups + g + 1) * head_dim)
            asked = [q[blocks[slot] * groups + g] for slot in at]
            scores = [
                lax.dot_general(
                    received[slot][:, key], ask, NN, preferred_element_type=jnp.float32
                )
                for slot, ask in zip(at, asked)
            ]
            tops = [jnp.max(score, axis=0, keepdims=True) for score in scores]
            raised = [jnp.exp(score - top) for score, top in zip(scores, tops)]
            totals = [jnp.sum(weight, axis=0, keepdims=True) for weight in raised]
            shares = [
                (weight * (1.0 / total)).astype(jnp.bfloat16)
                for weight, total in zip(raised, totals)
            ]
            parts = [
                lax.dot_general(
                    received[slot][:, value], share, TN, preferred_element_type=jnp.float32
                )
                for slot, share in zip(at, shares)
            ]
            for slot, part, top, total in zip(at, parts, tops, totals):
                partials[slot * groups + g] = part.astype(jnp.bfloat16)
                stats[slot * groups + g, 0:1, :] = top
                stats[slot * groups + g, 1:2, :] = total

    every(attend, steps, own=True)

    block_count = token_rows // block_rows
    parts = part_send.shape[0]
    part_blocks = block_count // parts
    part_rows = part_blocks * block_rows

    own_width = attended.shape[1] // 2
    own_columns = pl.multiple_of(core * own_width, own_width)

    def swap_part(k):
        here = attended.at[pl.ds(k * part_rows, part_rows), pl.ds(own_columns, own_width)]
        return remote(here, here, part_send.at[k], part_recv.at[k], across)

    def combine(b, carry):
        for g in range(groups):
            at = [slots[p * block_count + b] * groups + g for p in range(per_block)]
            tops = [stats[s, 0:1, :] for s in at]
            highest = functools.reduce(jnp.maximum, tops)
            scales = [jnp.exp(top - highest) * stats[s, 1:2, :] for top, s in zip(tops, at)]
            denominator = functools.reduce(jnp.add, scales)
            summed = functools.reduce(
                jnp.add, [partials[s].astype(jnp.float32) * scale for s, scale in zip(at, scales)]
            )
            done = jnp.transpose(summed * (1.0 / denominator)).astype(jnp.bfloat16)
            rows = pl.ds(pl.multiple_of(b * block_rows, block_rows), block_rows)
            for h in range(repeat):
                columns = pl.ds(own_columns + (g * repeat + h) * head_dim, head_dim)
                attended[rows, columns] = done[h * block_rows : (h + 1) * block_rows]
        return carry

    for k in range(parts):
        lax.fori_loop(k * part_blocks, (k + 1) * part_blocks, combine, 0)
        if k > 0:
            swap_part(k - 1).start()
    swap_part(parts - 1).start()

    def leave(k):
        rows = pl.ds(k * part_rows, part_rows)
        return pltpu.make_async_copy(
            normed.at[rows, pl.ds(0, conv.shape[1])], mixed_hbm.at[rows], out_sem.at[k]
        )

    for i in range(down_tiles):
        mine = range(i * parts // down_tiles, (i + 1) * parts // down_tiles)
        for k in mine:
            swap_part(k).wait_recv()
        rows = pl.ds(i * conv_rows, conv_rows)

        def project_out(c, carry, rows=rows):
            columns = pl.ds(pl.multiple_of(c * conv_columns, conv_columns), conv_columns)
            cross = jnp.dot(
                attended[rows, :], out_weight[:, columns], preferred_element_type=jnp.float32
            )
            gated = jax.nn.sigmoid(gate_logit[:, columns]) * cross
            normed[rows, columns] = (conv[rows, columns] + gated).astype(jnp.bfloat16)
            return carry

        lax.fori_loop(0, conv.shape[1] // conv_columns, project_out, 0)
        for k in mine:
            leave(k).start()
    every(lambda step, j: send_ids(step, j).wait_send(), steps)
    every(lambda step, j: send(0)(step, j).wait_send(), (0,))
    if relays:
        every(lambda step, j: send(1)(step, j).wait_send(), (0,))
        every(lambda step, j: send(2)(step, j).wait_send(), (0,))
        for c in range(chunks):
            hand(0, c).wait_send()

        @pl.when(middle)
        def _():
            for c in range(chunks):
                hand(1, c).wait_send()
                hand(2, c).wait_send()

        @pl.when(edge)
        def _():
            every(lambda step, j: send(0)(step, j).wait_send(), (2, 3))

    for k in range(parts):
        swap_part(k).wait_send()
        leave(k).wait()


def on_device(
    planes,
    tokens,
    norm_gain,
    branch_outer,
    branch_gate,
    branch_input,
    conv_taps,
    query_weight,
    query_gain,
    head_scale,
    store,
    store_gain,
    key_weight,
    value_weight,
    key_gain,
    out_weight,
    gate_logit,
    passage_ids,
):
    n = lax.axis_size("st")
    token_rows, local_width = tokens.shape
    head_dim = query_gain.shape[0]
    local_heads = query_weight.shape[1] // head_dim
    groups = key_weight.shape[1] // head_dim
    repeat = local_heads // groups
    block_count, per_block = passage_ids.shape
    block_rows = token_rows // block_count
    passages, passage_rows, width = store.shape
    channels = branch_outer.shape[1]
    requests = block_count * per_block
    capacity = max(2, (requests + n - 1) // n)
    count = n * capacity
    flat = passage_ids.T.reshape(requests)
    owners = flat // passages
    order = jnp.arange(requests, dtype=jnp.int32)
    earlier = (owners[:, None] == owners[None, :]) & (order[None, :] < order[:, None])
    slots = owners * capacity + jnp.sum(earlier.astype(jnp.int32), axis=1)
    lanes = LANES * ((count + LANES - 1) // LANES)
    filled = slots[None, :] == jnp.arange(lanes, dtype=jnp.int32)[:, None]
    pick = jnp.sum(jnp.where(filled, (flat - owners * passages)[None], 0), axis=1)
    blocks = jnp.sum(jnp.where(filled, lax.rem(order, block_count)[None], 0), axis=1)

    rows = passages * passage_rows
    chunks = largest(passages, (4, 2, 1))
    parts = largest(block_count, (4, 2, 1))
    pair_width = key_weight.shape[1] + value_weight.shape[1]
    wide = repeat * block_rows
    plane = n // planes
    relays = planes == 4
    buffers = 5 * plane if relays else plane
    bf16, f32 = jnp.bfloat16, jnp.float32
    dma = pltpu.SemaphoreType.DMA
    smem = pl.BlockSpec(memory_space=pltpu.SMEM)
    anywhere = pl.BlockSpec(memory_space=pl.ANY)
    cfg = (n, planes, capacity, per_block, groups, repeat, head_dim, block_rows)
    return pl.pallas_call(
        functools.partial(layer_kernel, cfg),
        out_shape=jax.ShapeDtypeStruct((token_rows, channels), bf16),
        in_specs=[smem] * 3 + [anywhere] * 16,
        out_specs=anywhere,
        scratch_shapes=[
            pltpu.VMEM((2, token_rows, local_width), bf16),
            pltpu.VMEM((token_rows, width), bf16),
            pltpu.VMEM((width, channels), bf16),
            pltpu.VMEM((width, channels), bf16),
            pltpu.VMEM((width, channels), bf16),
            pltpu.VMEM(query_weight.shape, bf16),
            pltpu.VMEM(out_weight.shape, bf16),
            pltpu.VMEM((width, pair_width), bf16),
            pltpu.VMEM((chunks, rows // chunks, width), bf16),
            pltpu.VMEM((passages, passage_rows, pair_width), bf16),
            pltpu.VMEM((passages if relays else 1, passage_rows, pair_width), bf16),
            pltpu.VMEM((passages if relays else 1, passage_rows, pair_width), bf16),
            pltpu.VMEM((buffers * capacity, passage_rows, pair_width), bf16),
            pltpu.VMEM((count, passage_rows, pair_width), bf16),
            pltpu.VMEM((block_count * groups, head_dim, wide), bf16),
            pltpu.VMEM((count * groups, head_dim, wide), bf16),
            pltpu.VMEM((count * groups, 2, wide), f32),
            pltpu.VMEM((token_rows, 2 * local_heads * head_dim), bf16),
            pltpu.VMEM((token_rows, channels), f32),
            pltpu.VMEM((1, width), f32),
            pltpu.VMEM(conv_taps.shape, f32),
            pltpu.VMEM((1, head_dim), f32),
            pltpu.VMEM((1, width), f32),
            pltpu.VMEM((1, head_dim), f32),
            pltpu.VMEM((1, channels), f32),
            pltpu.VMEM((1, lanes), jnp.int32),
            pltpu.VMEM((n, 1, lanes), jnp.int32),
            pltpu.SMEM((n, 1, lanes), jnp.int32),
            dma((chunks,)),
            dma((12,)),
            dma((5,)),
            dma((2,)),
            dma((n,)),
            dma((n,)),
            dma((3, chunks)),
            dma((2, chunks)),
            dma((buffers,)),
            dma((n,)),
            dma((parts,)),
            dma((parts,)),
            dma((parts,)),
        ],
        compiler_params=pltpu.CompilerParams(
            collective_id=0, has_side_effects=True, vmem_limit_bytes=62 * 1024 * 1024
        ),
        cost_estimate=pl.CostEstimate(
            flops=2 * token_rows * width * (3 * channels + local_heads * head_dim),
            bytes_accessed=8 * width * channels,
            transcendentals=0,
        ),
        name="layer",
    )(
        slots,
        blocks,
        head_scale,
        pick[None],
        tokens,
        norm_gain[None],
        branch_outer,
        branch_gate,
        branch_input,
        conv_taps,
        query_weight,
        query_gain[None],
        store.reshape(rows, width),
        store_gain[None],
        key_weight,
        value_weight,
        key_gain[None],
        out_weight,
        gate_logit[None],
    )


FIRST, SECOND = 2, 6


def planes_of(mesh):
    line = mesh.devices.reshape(mesh.shape["st"], -1)[:, 0]
    heights = [getattr(d, "coords", (0, 0, 0))[2] for d in line]
    planes = len(set(heights))
    plane = len(heights) // planes
    ordered = heights == [h for h in sorted(set(heights)) for _ in range(plane)]
    return planes if planes == 4 and ordered else 1


def solution(mesh):
    return jax.shard_map(
        functools.partial(on_device, planes_of(mesh)),
        mesh=mesh,
        in_specs=(
            P("st", "tp"),
            P(),
            P(None, "tp"),
            P(None, "tp"),
            P(None, "tp"),
            P(None, "tp"),
            P(None, "tp"),
            P(),
            P("tp"),
            P("st", None, None),
            P(),
            P(None, "tp"),
            P(None, "tp"),
            P(),
            P(None, "tp"),
            P("tp"),
            P("st", None),
        ),
        out_specs=P("st", "tp"),
        check_vma=False,
    )
```

time: 69.5 us -> 60.1 us (0.86)
  matrix products: 7.11 us -> 0 us
  Pallas kernels: 59.5 us -> 55.2 us
  local copies, waits for them, and re-layouts: 0.86 us -> 3.85 us
    dot_general x1 -> x0, matrix products: 7.11 us -> none  [on_device(): cross = jnp.dot(attended, out_weight, preferred_element_type=jnp.float32)]
    pallas_call x1, Pallas kernels: 59.5 us -> 55.2 us  [on_device(): pl.pallas_call(functools.partial(layer_kernel, cfg), out_shape=jax.ShapeD...]
    unnamed x3, local copies, waits for them, and re-layouts: 0.77 us -> 3.09 us
where the time goes in v1:
time: 60.1 us; the launch traced here: 59.9 us
  Pallas kernels  55.2 us (92%)
  local copies, waits for them, and re-layouts  3.85 us (6%)
  other arithmetic  0.85 us (1%)
    pallas_call x1, Pallas kernels, on_device(): pl.pallas_call(functools.partial(layer_kernel, cfg), out_shape=jax.ShapeD...  55.2 us
    unnamed x3, local copies, waits for them, and re-layouts  3.09 us

profile of v1, /device:TPU:1, one launch (start us, length us, event | category | flops | bytes accessed | tf_op | source)
XLA Modules:
  0.0 59.9 jit_solution(17609163107384989303)
XLA Ops:
  0.0 0.8 %reshape.93 = s32[64]{0:T(128)S(1)} reshape(s32[4,16]{1,0:T(4,128)} %bitcast.8) | data formatting | bytes 512 | tf_op jit(solution)/shard_map/reshape | solution.py:497
  0.8 0.2 convert_reduce_fusion
  1.0 0.0 copy-start
  1.0 0.7 %select_reduce_fusion = (s32[128]{0:T(128)}, s32[128]{0:T(128)}) fusion(s32[64]{0:T(128)S(1)} %get-tuple-element.7, s32[64]{0:T(128)S(1)} %multiply_add_fusion.slots, s32[64]{0:T(128)S(1)} %get-tuple-element.9), kind=kLoop, calls=%fused_computation | loop fusion | flops 40704 | bytes 1792 | tf_op jit(solution)/shard_map/reduce_sum | solution.py:504
  1.6 0.0 copy-done
  1.6 55.2 %layer.1 = bf16[1024,1024]{1,0:T(8,128)(2,1)} custom-call(s32[64]{0:T(128)} %copy-done, s32[128]{0:T(128)} %get-tuple-element.6.blocks, f32[4]{0:T(128)} %head_scale.1, s32[1,128]{1,0:T(1,128)} %bitcast.9, bf16[1024,1024]{1,0:T(8,128)(2,1)} %tokens_hbm.1, f32[1,2048]{1,0:T(1,128)} %bitcast.11, bf16[2048,1024]{1,0:T(8,128)(2,1)} %outer_hbm.1, ...), custom_call_target="tpu_custom_call" | custom-call | flops 15032385536 | bytes 16777216 | tf_op jit(solution)/shard_map/layer/pallas_call | solution.py:520
  56.8 3.1 %copy.19 = bf16[1024,1024]{1,0:T(8,128)(2,1)} copy(bf16[1024,1024]{1,0:T(8,128)(2,1)} %layer.1) | data formatting | bytes 4194304
  (2 shorter events, 0.0 us)
Async XLA Ops:
  1.0 0.7 %copy-start = (s32[64]{0:T(128)}, s32[64]{0:T(128)S(1)}, u32[]{:S(2)}) copy-start(s32[64]{0:T(128)S(1)} %multiply_add_fusion.slots) | copy-start | bytes 772

commit v2 on v1

--- a/solution.py
+++ b/solution.py
@@ -237,6 +237,7 @@
     listed = pltpu.make_async_copy(picks, wanted, side_sem.at[len(sides)])
     listed.start()
     listed.wait()
+    serve(0)
     if relays:
 
         @pl.when(edge)
@@ -244,7 +245,6 @@
             every(fill(0), (2, 3))
             every(lambda step, j: send(0)(step, j).start(), (2, 3))
 
-    serve(0)
 
     sides[-1].wait()
     swap_tokens.wait()
@@ -402,14 +402,15 @@
                 jnp.add, [partials[s].astype(jnp.float32) * scale for s, scale in zip(at, scales)]
             )
             done = jnp.transpose(summed * (1.0 / denominator)).astype(jnp.bfloat16)
-            rows = pl.ds(pl.multiple_of(b * block_rows, block_rows), block_rows)
+            rows = pl.ds(b * block_rows, block_rows)
             for h in range(repeat):
                 columns = pl.ds(own_columns + (g * repeat + h) * head_dim, head_dim)
                 attended[rows, columns] = done[h * block_rows : (h + 1) * block_rows]
         return carry
 
     for k in range(parts):
-        lax.fori_loop(k * part_blocks, (k + 1) * part_blocks, combine, 0)
+        for b in range(k * part_blocks, (k + 1) * part_blocks):
+            combine(b, 0)
         if k > 0:
             swap_part(k - 1).start()
     swap_part(parts - 1).start()
@@ -459,6 +460,44 @@
     for k in range(parts):
         swap_part(k).wait_send()
         leave(k).wait()
+
+
+def settle_kernel(source, target, held, load_sem, store_sem):
+    parts = load_sem.shape[0]
+    rows = source.shape[0] // parts
+
+    def load(k):
+        at = pl.ds(k * rows, rows)
+        return pltpu.make_async_copy(source.at[at], held.at[at], load_sem.at[k])
+
+    def store(k):
+        at = pl.ds(k * rows, rows)
+        return pltpu.make_async_copy(held.at[at], target.at[at], store_sem.at[k])
+
+    for k in range(parts):
+        load(k).start()
+    for k in range(parts):
+        load(k).wait()
+        store(k).start()
+    for k in range(parts):
+        store(k).wait()
+
+
+def settle(values):
+    parts = largest(values.shape[0] // 16, (8, 4, 2, 1))
+    return pl.pallas_call(
+        settle_kernel,
+        out_shape=jax.ShapeDtypeStruct(values.shape, values.dtype),
+        in_specs=[pl.BlockSpec(memory_space=pl.ANY)],
+        out_specs=pl.BlockSpec(memory_space=pl.ANY),
+        scratch_shapes=[
+            pltpu.VMEM(values.shape, values.dtype),
+            pltpu.SemaphoreType.DMA((parts,)),
+            pltpu.SemaphoreType.DMA((parts,)),
+        ],
+        compiler_params=pltpu.CompilerParams(vmem_limit_bytes=62 * 1024 * 1024),
+        name="settle",
+    )(values)
 
 
 def on_device(
@@ -517,7 +556,7 @@
     smem = pl.BlockSpec(memory_space=pltpu.SMEM)
     anywhere = pl.BlockSpec(memory_space=pl.ANY)
     cfg = (n, planes, capacity, per_block, groups, repeat, head_dim, block_rows)
-    return pl.pallas_call(
+    mixed = pl.pallas_call(
         functools.partial(layer_kernel, cfg),
         out_shape=jax.ShapeDtypeStruct((token_rows, channels), bf16),
         in_specs=[smem] * 3 + [anywhere] * 16,
@@ -595,6 +634,7 @@
         out_weight,
         gate_logit[None],
     )
+    return settle(mixed)
 
 
 FIRST, SECOND = 2, 6

time: 60.1 us -> 58.9 us (0.980)
  local copies, waits for them, and re-layouts: 3.85 us -> 0.77 us
  Pallas kernels: 55.2 us -> 56.8 us
    unnamed x3 -> x2, local copies, waits for them, and re-layouts: 3.09 us -> 0.01 us
    pallas_call x0 -> x1, Pallas kernels: none -> 2.39 us  [settle(): pl.pallas_call(settle_kernel, out_shape=jax.ShapeDtypeStruct(values.shape...]
    pallas_call x1, Pallas kernels: 55.2 us -> 54.4 us  [on_device(): pl.pallas_call(functools.partial(layer_kernel, cfg), out_shape=jax.ShapeD...]
where the time goes in v2:
time: 58.9 us; the launch traced here: 58.6 us
  Pallas kernels  56.8 us (96%)
  other arithmetic  0.85 us (1%)
  local copies, waits for them, and re-layouts  0.77 us (1%)
    pallas_call x1, Pallas kernels, on_device(): pl.pallas_call(functools.partial(layer_kernel, cfg), out_shape=jax.ShapeD...  54.4 us
    pallas_call x1, Pallas kernels, settle(): pl.pallas_call(settle_kernel, out_shape=jax.ShapeDtypeStruct(values.shape...  2.39 us

profile of v2, /device:TPU:1, one launch (start us, length us, event | category | flops | bytes accessed | tf_op | source)
XLA Modules:
  0.0 58.6 jit_solution(5934180846278536345)
XLA Ops:
  0.0 0.8 %reshape.93 = s32[64]{0:T(128)S(1)} reshape(s32[4,16]{1,0:T(4,128)} %bitcast.8) | data formatting | bytes 512 | tf_op jit(solution)/shard_map/reshape | solution.py:536
  0.8 0.2 convert_reduce_fusion
  1.0 0.0 copy-start
  1.0 0.7 %select_reduce_fusion = (s32[128]{0:T(128)}, s32[128]{0:T(128)}) fusion(s32[64]{0:T(128)S(1)} %get-tuple-element.7, s32[64]{0:T(128)S(1)} %multiply_add_fusion.slots, s32[64]{0:T(128)S(1)} %get-tuple-element.9), kind=kLoop, calls=%fused_computation | loop fusion | flops 40704 | bytes 1792 | tf_op jit(solution)/shard_map/reduce_sum | solution.py:543
  1.6 0.0 copy-done
  1.6 54.4 %layer.1.source = bf16[1024,1024]{1,0:T(8,128)(2,1)} custom-call(s32[64]{0:T(128)} %copy-done, s32[128]{0:T(128)} %get-tuple-element.6.blocks, f32[4]{0:T(128)} %head_scale.1, s32[1,128]{1,0:T(1,128)} %bitcast.9, bf16[1024,1024]{1,0:T(8,128)(2,1)} %tokens_hbm.1, f32[1,2048]{1,0:T(1,128)} %bitcast.11, bf16[2048,1024]{1,0:T(8,128)(2,1)} %outer_hbm.1, ...), custom_call_target="tpu_custom_call" | custom-call | flops 15032385536 | bytes 16777216 | tf_op jit(solution)/shard_map/layer/pallas_call | solution.py:559
  56.1 2.4 %settle.1 = bf16[1024,1024]{1,0:T(8,128)(2,1)} custom-call(bf16[1024,1024]{1,0:T(8,128)(2,1)} %layer.1.source), custom_call_target="tpu_custom_call" | custom-call | tf_op jit(solution)/shard_map/settle/pallas_call | solution.py:488
  (2 shorter events, 0.0 us)
Async XLA Ops:
  1.0 0.7 %copy-start = (s32[64]{0:T(128)}, s32[64]{0:T(128)S(1)}, u32[]{:S(2)}) copy-start(s32[64]{0:T(128)S(1)} %multiply_add_fusion.slots) | copy-start | bytes 772

commit v3 on v2

--- a/solution.py
+++ b/solution.py
@@ -415,10 +415,13 @@
             swap_part(k - 1).start()
     swap_part(parts - 1).start()
 
-    def leave(k):
-        rows = pl.ds(k * part_rows, part_rows)
+    across_tiles = conv_tiles // down_tiles
+
+    def leave(i, c):
+        rows = pl.ds(i * conv_rows, conv_rows)
+        columns = pl.ds(pl.multiple_of(c * conv_columns, conv_columns), conv_columns)
         return pltpu.make_async_copy(
-            normed.at[rows, pl.ds(0, conv.shape[1])], mixed_hbm.at[rows], out_sem.at[k]
+            normed.at[rows, columns], mixed_hbm.at[rows, columns], out_sem.at[i * across_tiles + c]
         )
 
     for i in range(down_tiles):
@@ -427,18 +430,17 @@
             swap_part(k).wait_recv()
         rows = pl.ds(i * conv_rows, conv_rows)
 
-        def project_out(c, carry, rows=rows):
+        def project_out(c, carry, rows=rows, i=i):
             columns = pl.ds(pl.multiple_of(c * conv_columns, conv_columns), conv_columns)
             cross = jnp.dot(
                 attended[rows, :], out_weight[:, columns], preferred_element_type=jnp.float32
             )
             gated = jax.nn.sigmoid(gate_logit[:, columns]) * cross
             normed[rows, columns] = (conv[rows, columns] + gated).astype(jnp.bfloat16)
+            leave(i, c).start()
             return carry
 
-        lax.fori_loop(0, conv.shape[1] // conv_columns, project_out, 0)
-        for k in mine:
-            leave(k).start()
+        lax.fori_loop(0, across_tiles, project_out, 0)
     every(lambda step, j: send_ids(step, j).wait_send(), steps)
     every(lambda step, j: send(0)(step, j).wait_send(), (0,))
     if relays:
@@ -459,7 +461,9 @@
 
     for k in range(parts):
         swap_part(k).wait_send()
-        leave(k).wait()
+    for i in range(down_tiles):
+        for c in range(across_tiles):
+            leave(i, c).wait()
 
 
 def settle_kernel(source, target, held, load_sem, store_sem):
@@ -548,6 +552,9 @@
     parts = largest(block_count, (4, 2, 1))
     pair_width = key_weight.shape[1] + value_weight.shape[1]
     wide = repeat * block_rows
+    tiles = (token_rows // (largest(token_rows // SEQ, (4, 2, 1)) * SEQ)) * (
+        channels // (largest(channels // LANES, (2, 1)) * LANES)
+    )
     plane = n // planes
     relays = planes == 4
     buffers = 5 * plane if relays else plane
@@ -602,7 +609,7 @@
             dma((n,)),
             dma((parts,)),
             dma((parts,)),
-            dma((parts,)),
+            dma((tiles,)),
         ],
         compiler_params=pltpu.CompilerParams(
             collective_id=0, has_side_effects=True, vmem_limit_bytes=62 * 1024 * 1024

time: 58.9 us -> 58.6 us (level)
  no operation moved by 1% of the time
where the time goes in v3:
time: 58.6 us; the launch traced here: 58.4 us
  Pallas kernels  56.6 us (97%)
  other arithmetic  0.85 us (1%)
  local copies, waits for them, and re-layouts  0.77 us (1%)
    pallas_call x1, Pallas kernels, on_device(): pl.pallas_call(functools.partial(layer_kernel, cfg), out_shape=jax.ShapeD...  54.2 us
    pallas_call x1, Pallas kernels, settle(): pl.pallas_call(settle_kernel, out_shape=jax.ShapeDtypeStruct(values.shape...  2.39 us

profile of v3, /device:TPU:1, one launch (start us, length us, event | category | flops | bytes accessed | tf_op | source)
XLA Modules:
  0.0 58.4 jit_solution(2479739757028244862)
XLA Ops:
  0.0 0.8 %reshape.93 = s32[64]{0:T(128)S(1)} reshape(s32[4,16]{1,0:T(4,128)} %bitcast.8) | data formatting | bytes 512 | tf_op jit(solution)/shard_map/reshape | solution.py:540
  0.8 0.2 convert_reduce_fusion
  1.0 0.0 copy-start
  1.0 0.7 %select_reduce_fusion = (s32[128]{0:T(128)}, s32[128]{0:T(128)}) fusion(s32[64]{0:T(128)S(1)} %get-tuple-element.7, s32[64]{0:T(128)S(1)} %multiply_add_fusion.slots, s32[64]{0:T(128)S(1)} %get-tuple-element.9), kind=kLoop, calls=%fused_computation | loop fusion | flops 40704 | bytes 1792 | tf_op jit(solution)/shard_map/reduce_sum | solution.py:547
  1.6 0.0 copy-done
  1.6 54.2 %layer.1.source = bf16[1024,1024]{1,0:T(8,128)(2,1)} custom-call(s32[64]{0:T(128)} %copy-done, s32[128]{0:T(128)} %get-tuple-element.6.blocks, f32[4]{0:T(128)} %head_scale.1, s32[1,128]{1,0:T(1,128)} %bitcast.9, bf16[1024,1024]{1,0:T(8,128)(2,1)} %tokens_hbm.1, f32[1,2048]{1,0:T(1,128)} %bitcast.11, bf16[2048,1024]{1,0:T(8,128)(2,1)} %outer_hbm.1, ...), custom_call_target="tpu_custom_call" | custom-call | flops 15032385536 | bytes 16777216 | tf_op jit(solution)/shard_map/layer/pallas_call | solution.py:566
  55.8 2.4 %settle.1 = bf16[1024,1024]{1,0:T(8,128)(2,1)} custom-call(bf16[1024,1024]{1,0:T(8,128)(2,1)} %layer.1.source), custom_call_target="tpu_custom_call" | custom-call | tf_op jit(solution)/shard_map/settle/pallas_call | solution.py:492
  (2 shorter events, 0.0 us)
Async XLA Ops:
  1.0 0.7 %copy-start = (s32[64]{0:T(128)}, s32[64]{0:T(128)S(1)}, u32[]{:S(2)}) copy-start(s32[64]{0:T(128)S(1)} %multiply_add_fusion.slots) | copy-start | bytes 772
